TPU v7x, 32 devices: a whole 2x2x4 slice. The times are simulated.
32 devices in a mesh: rep: 2 (over x), fs: 8 (over z, y), tp: 2 (over core).
Axes of the slice: x: 2, y: 2, z: 4, core: 2. Of those that a mesh axis runs over, the one named last changes fastest.
Arguments:
- tokens: bfloat16 [8192, 2048], P(('rep', 'fs', 'tp')), may hold values from -6 to 6
- norm_gain: float32 [2048], replicated, may hold values from 0.1 to 1.9
- gate_weight: float32 [2048, 5120], P('fs', 'tp'), may hold values from -0.125 to 0.125
- gate_scale: float32 [5120], P('tp'), may hold values from 0.1 to 1.9
- up_weight: float32 [2048, 5120], P('fs', 'tp'), may hold values from -0.125 to 0.125
- up_scale: float32 [5120], P('tp'), may hold values from 0.1 to 1.9
- down_weight: float32 [5120, 2048], P('tp', 'fs'), may hold values from -0.078125 to 0.078125
- down_scale: float32 [2048], replicated, may hold values from 0.1 to 1.9
Outputs:
- mixed: bfloat16 [8192, 2048], P(('rep', 'fs', 'tp'))
All inputs are finite; a program needn't handle non-finite values.
Results may differ from a plain program's by a relative error of at most 0.013.
Values may be sent and summed in bfloat16 or wider, within the bound.
A program may use at most 128 MiB of HBM per device.

v0:
```python
import jax
import jax.numpy as jnp
from jax import lax
from jax.sharding import PartitionSpec as P

EPS_VALUE = 1e-06


def from_partner(shard, axis, distance):
    return lax.ppermute(shard, axis, [(i, i ^ 1 << distance) for i in range(lax.axis_size(axis))])


def normalize(token_rows, norm_gain):
    values = token_rows.astype(jnp.float32)
    inverse = lax.rsqrt(jnp.mean(values * values, axis=-1, keepdims=True) + EPS_VALUE)
    return (values * inverse * norm_gain).astype(jnp.bfloat16)


def body(tokens, norm_gain, gate_weight, gate_scale, up_weight, up_scale, down_weight, down_scale):
    normed = normalize(tokens, norm_gain)
    gate_bf = gate_weight.astype(jnp.bfloat16)
    up_bf = up_weight.astype(jnp.bfloat16)
    down_bf = down_weight.astype(jnp.bfloat16)
    rep_index = lax.axis_index("rep")
    half_cols = gate_bf.shape[1] // 2
    half_rows = down_bf.shape[0] // 2
    own_gate = lax.dynamic_slice_in_dim(gate_bf, rep_index * half_cols, half_cols, 1)
    own_up = lax.dynamic_slice_in_dim(up_bf, rep_index * half_cols, half_cols, 1)
    own_down = lax.dynamic_slice_in_dim(down_bf, rep_index * half_rows, half_rows, 0)
    own_parts = (
        lax.all_gather(own_gate, "fs", axis=0, tiled=True),
        lax.all_gather(own_up, "fs", axis=0, tiled=True),
        lax.all_gather(own_down, "fs", axis=1, tiled=True),
    )
    far_parts = from_partner((own_parts[0], own_parts[1], own_parts[2]), "rep", 0)
    is_first = rep_index == 0

    def joined(own_part, far_part, axis_dim):
        return jnp.where(
            is_first,
            jnp.concatenate([own_part, far_part], axis_dim),
            jnp.concatenate([far_part, own_part], axis_dim),
        )

    gate_full = joined(own_parts[0], far_parts[0], 1)
    up_full = joined(own_parts[1], far_parts[1], 1)
    down_full = joined(own_parts[2], far_parts[2], 0)
    slab_rows = lax.all_gather(normed, "tp", axis=0, tiled=True)
    gate_pre = jnp.dot(slab_rows, gate_full, preferred_element_type=jnp.float32) * gate_scale
    up_pre = jnp.dot(slab_rows, up_full, preferred_element_type=jnp.float32) * up_scale
    hidden = (jax.nn.silu(gate_pre) * up_pre).astype(jnp.bfloat16)
    partial_value = (
        jnp.dot(hidden, down_full, preferred_element_type=jnp.float32) * down_scale
    ).astype(jnp.bfloat16)
    partial_value = lax.optimization_barrier(partial_value)
    return lax.psum_scatter(
        partial_value.astype(jnp.float32).astype(jnp.bfloat16),
        "tp",
        scatter_dimension=0,
        tiled=True,
    )


def solution(mesh):
    return jax.shard_map(
        body,
        mesh=mesh,
        in_specs=(
            P(("rep", "fs", "tp"), None),
            P(),
            P("fs", "tp"),
            P("tp"),
            P("fs", "tp"),
            P("tp"),
            P("tp", "fs"),
            P(),
        ),
        out_specs=P(("rep", "fs", "tp"), None),
        check_vma=False,
    )
```

profile of v0, /device:TPU:1, one launch (start us, length us, event | category | flops | bytes accessed | tf_op | source)
XLA Modules:
  0.0 482.0 jit_solution(2602292842199333268)
XLA Ops:
  7.4 1.7 copy-done
  9.1 0.9 dynamic-slice_convert_fusion.2
  10.1 0.0 all-gather.9.cloned.1.call-start
  10.1 2.2 dynamic-slice_convert_fusion.1
  12.4 0.0 all-gather.11.cloned.1.call-start
  12.4 2.2 dynamic-slice_convert_fusion
  14.7 0.0 all-gather.5.cloned.1.call-start
  14.7 82.1 %all-gather.7.cloned.1.call-done = bf16[2048,1280]{1,0:T(8,128)(2,1)} async-done(((bf16[256,1280]{1,0:T(8,128)(2,1)}), bf16[2048,1280]{1,0:T(8,128)(2,1)}) %all-gather.7.cloned.1.call-update) | async-done | bytes 5242896 | tf_op jit(solution)/shard_map/all_gather | solution.py:31
  96.8 1.2 collective-permute-start
  98.0 85.1 %all-gather.9.cloned.1.call-done = bf16[2048,1280]{1,0:T(8,128)(2,1)} async-done(((bf16[256,1280]{1,0:T(8,128)(2,1)}), bf16[2048,1280]{1,0:T(8,128)(2,1)}) %all-gather.9.cloned.1.call-update) | async-done | bytes 5242896 | tf_op jit(solution)/shard_map/all_gather | solution.py:32
  183.0 1.2 collective-permute-start.1
  184.2 86.7 %all-gather.11.cloned.1.call-done = bf16[1280,2048]{1,0:T(8,128)(2,1)} async-done(((bf16[1280,256]{1,0:T(8,128)(2,1)}), bf16[1280,2048]{1,0:T(8,128)(2,1)}) %all-gather.11.cloned.1.call-update) | async-done | bytes 5242896 | tf_op jit(solution)/shard_map/all_gather | solution.py:33
  270.9 1.3 collective-permute-start.2
  272.2 1.5 fusion.21
  273.7 2.5 fusion.23
  276.2 0.0 all-gather.5.cloned.1.call-update
  276.2 0.0 reduce-scatter.2.cloned.1.call-start
  276.3 9.1 %all-gather.5.cloned.1.call-done = bf16[512,2048]{1,0:T(8,128)(2,1)} async-done(((bf16[256,2048]{1,0:T(8,128)(2,1)}), bf16[512,2048]{1,0:T(8,128)(2,1)}) %all-gather.5.cloned.1.call-update) | async-done | bytes 2097168 | tf_op jit(solution)/shard_map/all_gather | solution.py:48
  285.4 15.7 %fusion = f32[512,2560]{1,0:T(8,128)} fusion(bf16[512,2048]{1,0:T(8,128)(2,1)} %all-gather.5.cloned.1.call-done, bf16[2048,1280]{1,0:T(8,128)(2,1)} %collective-permute-done, bf16[2048,1280]{1,0:T(8,128)(2,1)} %all-gather.7.cloned.1.call-done, pred[]{:T(512)S(6)} %eq.3), kind=kOutput, calls=%fused_computation.1 | convolution fusion | flops 5415895040 | bytes 17825792 | tf_op jit(solution)/shard_map/dot_general | solution.py:49
  301.1 20.7 %collective-permute-done.1 = bf16[2048,1280]{1,0:T(8,128)(2,1)} collective-permute-done((bf16[2048,1280]{1,0:T(8,128)(2,1)}, bf16[2048,1280]{1,0:T(8,128)(2,1)}, u32[]{:S(2)}, u32[]{:S(2)}) %collective-permute-start.1) | collective-permute-done | bytes 5242912 | tf_op jit(solution)/shard_map/ppermute | solution.py:10
  321.8 112.4 %collective-permute-done.2 = bf16[1280,2048]{1,0:T(8,128)(2,1)} collective-permute-done((bf16[1280,2048]{1,0:T(8,128)(2,1)}, bf16[1280,2048]{1,0:T(8,128)(2,1)}, u32[]{:S(2)}, u32[]{:S(2)}) %collective-permute-start.2) | collective-permute-done | bytes 5242912 | tf_op jit(solution)/shard_map/ppermute | solution.py:10
  434.2 28.2 %multiply_convert_fusion.1 = bf16[512,2048]{1,0:T(8,128)(2,1)} fusion(bf16[1280,2048]{1,0:T(8,128)(2,1)} %collective-permute-done.2, bf16[1280,2048]{1,0:T(8,128)(2,1)} %all-gather.11.cloned.1.call-done, pred[]{:T(512)S(6)} %eq.3, f32[2048]{0:T(1024)S(1)} %copy-done.4, f32[512,2560]{1,0:T(8,128)} %fusion, ...), kind=kOutput, calls=%fused_computation.25 | convolution fusion | flops 10844372992 | bytes 30437376 | tf_op jit(solution)/shard_map/dot_general | solution.py:53
  462.4 0.0 reduce-scatter.2.cloned.1.call-update
  462.4 12.5 %reduce-scatter.2.cloned.1.call-done = bf16[256,2048]{1,0:T(8,128)(2,1)} async-done(((bf16[512,2048]{1,0:T(8,128)(2,1)}), bf16[256,2048]{1,0:T(8,128)(2,1)}) %reduce-scatter.2.cloned.1.call-update) | async-done | bytes 1048592 | tf_op jit(solution)/shard_map/reduce_scatter | solution.py:56
  (15 shorter events, 0.1 us)
Async XLA Ops:
  7.4 1.7 copy-start
  7.4 266.3 %copy-start.1 = (f32[2048]{0:T(1024)S(1)}, f32[2048]{0:T(1024)}, u32[]{:S(2)}) copy-start(f32[2048]{0:T(1024)} %param.9) | copy-start | bytes 24580
  7.4 89.4 %all-gather.7.cloned.1.call-start = ((), (), s32[]{:S(2)}) async-start(), calls=%async_computation.2 | async-start | bytes 5898240 | tf_op jit(solution)/shard_map/all_gather | solution.py:31
  10.1 173.0 %all-gather.9.cloned.1.call-start = ((), (), s32[]{:S(2)}) async-start(), calls=%async_computation.3 | async-start | bytes 5898240 | tf_op jit(solution)/shard_map/all_gather | solution.py:32
  12.4 258.5 %all-gather.11.cloned.1.call-start = ((), (), s32[]{:S(2)}) async-start(), calls=%async_computation.4 | async-start | bytes 5898240 | tf_op jit(solution)/shard_map/all_gather | solution.py:33
  14.7 270.7 %all-gather.5.cloned.1.call-start = ((), (), s32[]{:S(2)}) async-start(), calls=%async_computation.1 | async-start | bytes 3145728 | tf_op jit(solution)/shard_map/all_gather | solution.py:48
  96.8 188.6 %collective-permute-start = (bf16[2048,1280]{1,0:T(8,128)(2,1)}, bf16[2048,1280]{1,0:T(8,128)(2,1)}, u32[]{:S(2)}, u32[]{:S(2)}) collective-permute-start(bf16[2048,1280]{1,0:T(8,128)(2,1)} %all-gather.7.cloned.1.call-done), channel_id=1, source_target_pairs={{0,16},{16,0},{1,17},{17,1},{2,18},{18,2},{3,19},{19,3},{4,20},{20... | collective-permute-start | bytes 15728648 | tf_op jit(solution)/shard_map/ppermute | solution.py:10
  183.0 138.7 %collective-permute-start.1 = (bf16[2048,1280]{1,0:T(8,128)(2,1)}, bf16[2048,1280]{1,0:T(8,128)(2,1)}, u32[]{:S(2)}, u32[]{:S(2)}) collective-permute-start(bf16[2048,1280]{1,0:T(8,128)(2,1)} %all-gather.9.cloned.1.call-done), channel_id=1, source_target_pairs={{0,16},{16,0},{1,17},{17,1},{2,18},{18,2},{3,19},{19,3},{4,20},{20... | collective-permute-start | bytes 15728648 | tf_op jit(solution)/shard_map/ppermute | solution.py:10
  270.9 163.3 %collective-permute-start.2 = (bf16[1280,2048]{1,0:T(8,128)(2,1)}, bf16[1280,2048]{1,0:T(8,128)(2,1)}, u32[]{:S(2)}, u32[]{:S(2)}) collective-permute-start(bf16[1280,2048]{1,0:T(8,128)(2,1)} %all-gather.11.cloned.1.call-done), channel_id=1, source_target_pairs={{0,16},{16,0},{1,17},{17,1},{2,18},{18,2},{3,19},{19,3},{4,20},{20... | collective-permute-start | bytes 15728648 | tf_op jit(solution)/shard_map/ppermute | solution.py:10
  276.2 198.6 %reduce-scatter.2.cloned.1.call-start = ((), (), s32[]{:S(2)}) async-start(), calls=%async_computation.5 | async-start | bytes 3145728 | tf_op jit(solution)/shard_map/reduce_scatter | solution.py:56
  276.3 157.9 %copy-start.2 = (f32[2560]{0:T(1024)S(1)}, f32[2560]{0:T(1024)}, u32[]{:S(2)}) copy-start(f32[2560]{0:T(1024)} %param.13) | copy-start | bytes 30724
  276.3 157.9 %copy-start.3 = (f32[2560]{0:T(1024)S(1)}, f32[2560]{0:T(1024)}, u32[]{:S(2)}) copy-start(f32[2560]{0:T(1024)} %param.11) | copy-start | bytes 30724
  276.3 157.8 %copy-start.4 = (f32[2048]{0:T(1024)S(1)}, f32[2048]{0:T(1024)}, u32[]{:S(2)}) copy-start(f32[2048]{0:T(1024)} %param.15) | copy-start | bytes 24580
Sparse Core Ops, SparseCore 0:
  10.4 86.3 all-gather.6
  98.9 84.0 all-gather.8
  185.1 85.7 all-gather.10
Sparse Core Ops, SparseCore 1:
  276.3 9.0 all-gather.4
  462.5 12.3 reduce-scatter.1
where the time goes:
time: 482 us
  waiting for transfers between devices  408 us (85%)
  matrix products  43.9 us (9%)
  between operations  14.6 us (3%)
  local copies, waits for them, and re-layouts  7.14 us (1%)
    ppermute x3, waiting for transfers between devices, from_partner(): lax.ppermute(shard, axis, [(i, i ^ 1 << distance) for i in range(lax.axis...  133 us
    all_gather x1, waiting for transfers between devices, body(): lax.all_gather(own_down, 'fs', axis=1, tiled=True)  86.7 us
    all_gather x1, waiting for transfers between devices, body(): lax.all_gather(own_up, 'fs', axis=0, tiled=True)  85.1 us
    all_gather x1, waiting for transfers between devices, body(): lax.all_gather(own_gate, 'fs', axis=0, tiled=True)  82.1 us
    dot_general x1, matrix products, body(): jnp.dot(hidden, down_full, preferred_element_type=jnp.float32) * down_scale  28.2 us
    dot_general x1, matrix products, body(): jnp.dot(slab_rows, gate_full, preferred_element_type=jnp.float32)  15.7 us
    reduce_scatter x1, waiting for transfers between devices, body(): lax.psum_scatter(partial_value.astype(jnp.float32).astype(jnp.bfloat16),...  12.5 us
  transfers between devices with their start and end apart: 8, of which 7 were waited for; matrix products, arithmetic and copies ran while one was open for 5% of the time, Pallas kernels for 0%

commit v1 on v0

--- a/solution.py
+++ b/solution.py
@@ -1,6 +1,10 @@
+import functools
+
 import jax
 import jax.numpy as jnp
 from jax import lax
+from jax.experimental import pallas as pl
+from jax.experimental.pallas import tpu as pltpu
 from jax.sharding import PartitionSpec as P
 
 EPS_VALUE = 1e-06
@@ -61,20 +65,327 @@
     )
 
 
+MESH = pl.DeviceIdType.MESH
+
+
+def ffn_kernel(
+    sizes, tok_ref, gain_ref, gate_ref, gscale_ref, up_ref, uscale_ref, down_ref, dscale_ref, out_ref,
+    wg, wu, wd, rows_x, acc_g, acc_u, hid, staged, landed,
+    copy_sem, ring_send, ring_recv, down_send, down_recv, tok_send, tok_recv, part_send, part_recv,
+):
+    n_rep, n_fs, n_tp = sizes
+    group = n_rep * n_tp
+    steps = n_fs - 1
+    half_ring = n_fs // 2
+    n_tok, width = tok_ref.shape
+    depth = wg.shape[1]
+    half_depth = depth // 2
+    cols = wd.shape[3]
+    half_hid = wd.shape[2] // 2
+
+    rep = lax.axis_index("rep")
+    fs = lax.axis_index("fs")
+    tp = lax.axis_index("tp")
+    member = rep * n_tp + tp
+
+    side = fs % 2
+    place = (1 - side) * (fs // 2) + side * (n_fs - 1 - fs // 2)
+
+    def fs_at(position):
+        spot = (position + 2 * n_fs) % n_fs
+        back = spot // half_ring
+        return (1 - back) * 2 * spot + back * (2 * (n_fs - 1 - spot) + 1)
+
+    right = (rep, fs_at(place + 1), tp)
+    left = (rep, fs_at(place - 1), tp)
+
+    def peer(offset):
+        other = (member + offset) % group
+        return other, (other // n_tp, fs, other % n_tp)
+
+    def origin(direction, hops):
+        return fs_at(place - hops) if direction == 0 else fs_at(place + hops)
+
+    def ring_copy(direction, piece, step):
+        store = wg if direction == 0 else wu
+        part = store.at[origin(direction, step), pl.ds(piece * half_depth, half_depth)]
+        return pltpu.make_async_remote_copy(
+            src_ref=part, dst_ref=part,
+            send_sem=ring_send.at[direction, piece, step], recv_sem=ring_recv.at[direction, piece, step],
+            device_id=right if direction == 0 else left, device_id_type=MESH,
+        )
+
+    def ring_arrival(direction, piece, step):
+        store = wg if direction == 0 else wu
+        part = store.at[origin(direction, step + 1), pl.ds(piece * half_depth, half_depth)]
+        return pltpu.make_async_remote_copy(
+            src_ref=part, dst_ref=part,
+            send_sem=ring_send.at[direction, piece, step], recv_sem=ring_recv.at[direction, piece, step],
+            device_id=right if direction == 0 else left, device_id_type=MESH,
+        )
+
+    def down_copy(direction, piece, step, hops):
+        part = wd.at[origin(direction, hops), direction, pl.ds(piece * half_hid, half_hid)]
+        return pltpu.make_async_remote_copy(
+            src_ref=part, dst_ref=part,
+            send_sem=down_send.at[direction, piece, step], recv_sem=down_recv.at[direction, piece, step],
+            device_id=right if direction == 0 else left, device_id_type=MESH,
+        )
+
+    def token_copy(offset, slot):
+        return pltpu.make_async_remote_copy(
+            src_ref=rows_x.at[slot], dst_ref=rows_x.at[slot],
+            send_sem=tok_send.at[offset - 1], recv_sem=tok_recv.at[offset - 1],
+            device_id=peer(offset)[1], device_id_type=MESH,
+        )
+
+    def part_copy(offset, index):
+        other, where = peer(offset)
+        return pltpu.make_async_remote_copy(
+            src_ref=staged.at[index, other], dst_ref=landed.at[index, offset - 1],
+            send_sem=part_send.at[index, offset - 1], recv_sem=part_recv.at[index, offset - 1],
+            device_id=where, device_id_type=MESH,
+        )
+
+    own = [
+        pltpu.make_async_copy(gate_ref, wg.at[fs], copy_sem.at[0]),
+        pltpu.make_async_copy(up_ref, wu.at[fs], copy_sem.at[1]),
+        pltpu.make_async_copy(down_ref.at[:, pl.ds(0, cols)], wd.at[fs, 0], copy_sem.at[2]),
+        pltpu.make_async_copy(down_ref.at[:, pl.ds(cols, cols)], wd.at[fs, 1], copy_sem.at[3]),
+    ]
+    for copy in own:
+        copy.start()
+    barrier = pltpu.get_barrier_semaphore()
+    for device in [right, left] + [peer(offset)[1] for offset in range(1, group)]:
+        pl.semaphore_signal(barrier, inc=1, device_id=device, device_id_type=MESH)
+    pl.semaphore_wait(barrier, group + 1)
+    own[0].wait()
+    own[1].wait()
+    for piece in range(2):
+        for direction in range(2):
+            ring_copy(direction, piece, 0).start()
+
+    values = tok_ref[...].astype(jnp.float32)
+    inverse = lax.rsqrt(jnp.mean(values * values, axis=-1, keepdims=True) + EPS_VALUE)
+    rows_x[member] = (values * inverse * gain_ref[...]).astype(jnp.bfloat16)
+    own[2].wait()
+    own[3].wait()
+    for offset in range(1, group):
+        token_copy(offset, member).start()
+
+    def add_slice(index):
+        gate_fs, up_fs = origin(0, index), origin(1, index)
+        gate_cols = pl.ds(pl.multiple_of(gate_fs * depth, depth), depth)
+        up_cols = pl.ds(pl.multiple_of(up_fs * depth, depth), depth)
+
+        def tile(block, carry):
+            gate_term = jnp.dot(rows_x[block, :, gate_cols], wg[gate_fs], preferred_element_type=jnp.float32)
+            up_term = jnp.dot(rows_x[block, :, up_cols], wu[up_fs], preferred_element_type=jnp.float32)
+
+            @pl.when(index == 0)
+            def _():
+                acc_g[block] = gate_term
+                acc_u[block] = up_term
+
+            @pl.when(index > 0)
+            def _():
+                acc_g[block] += gate_term
+                acc_u[block] += up_term
+
+            return carry
+
+        lax.fori_loop(0, group, tile, 0)
+
+    def ring_step(step, carry):
+        for piece in range(2):
+            for direction in range(2):
+                ring_arrival(direction, piece, step).wait_recv()
+
+                @pl.when(step < steps - 1)
+                def _():
+                    ring_copy(direction, piece, step + 1).start()
+
+        @pl.when(step == steps - 3)
+        def _():
+            for piece in range(2):
+                for direction in range(2):
+                    down_copy(direction, piece, 0, 0).start()
+
+        @pl.when(step == half_ring - 1)
+        def _():
+            for offset in range(1, group):
+                token_copy(offset, (member + group - offset) % group).wait_recv()
+
+        @pl.when(step == steps - 1)
+        def _():
+            for piece in range(2):
+                for direction in range(2):
+                    down_copy(direction, piece, 0, 1).wait_recv()
+                    down_copy(direction, piece, 1, 1).start()
+
+        @pl.when(step >= half_ring - 1)
+        def _():
+            first = 2 * (step - (half_ring - 1))
+
+            def one(extra, inner):
+                add_slice(first + extra)
+                return inner
+
+            lax.fori_loop(0, 2, one, 0)
+
+        return carry
+
+    lax.fori_loop(0, steps, ring_step, 0)
+
+    def activate(block, carry):
+        gate_pre = acc_g[block] * gscale_ref[...]
+        up_pre = acc_u[block] * uscale_ref[...]
+        hid[block] = (jax.nn.silu(gate_pre) * up_pre).astype(jnp.bfloat16)
+        return carry
+
+    lax.fori_loop(0, group, activate, 0)
+
+    def produce(hops):
+        for direction in range(2):
+            source = origin(direction, hops)
+            start = pl.multiple_of(source * 2 * cols + direction * cols, cols)
+            scale = dscale_ref[:, pl.ds(start, cols)]
+            index = 2 * hops + direction
+
+            def tile(block, carry):
+                product = jnp.dot(hid[block], wd[source, direction], preferred_element_type=jnp.float32)
+                staged[index, block] = (product * scale).astype(jnp.bfloat16)
+                return carry
+
+            lax.fori_loop(0, group, tile, 0)
+            for offset in range(1, group):
+                part_copy(offset, index).start()
+
+    def down_step(step, carry):
+        @pl.when((step >= 2) & (step <= steps))
+        def _():
+            for piece in range(2):
+                for direction in range(2):
+                    down_copy(direction, piece, step - 1, step).wait_recv()
+
+                    @pl.when(step < steps)
+                    def _():
+                        down_copy(direction, piece, step, step).start()
+
+        produce(step)
+        return carry
+
+    lax.fori_loop(0, n_fs, down_step, 0)
+
+    def finish(hops, carry):
+        for direction in range(2):
+            index = 2 * hops + direction
+            total = staged[index, member].astype(jnp.float32)
+            for offset in range(1, group):
+                part_copy(offset, index).wait_recv()
+                total = total + landed[index, offset - 1].astype(jnp.float32)
+            start = pl.multiple_of(origin(direction, hops) * 2 * cols + direction * cols, cols)
+            out_ref[:, pl.ds(start, cols)] = total.astype(out_ref.dtype)
+        return carry
+
+    lax.fori_loop(0, n_fs, finish, 0)
+
+    def drain(step, carry):
+        for piece in range(2):
+            for direction in range(2):
+                ring_copy(direction, piece, step).wait_send()
+                down_copy(direction, piece, step, step).wait_send()
+        return carry
+
+    lax.fori_loop(0, steps, drain, 0)
+
+    def drain_parts(index, carry):
+        for offset in range(1, group):
+            part_copy(offset, index).wait_send()
+        return carry
+
+    lax.fori_loop(0, 2 * n_fs, drain_parts, 0)
+    for offset in range(1, group):
+        token_copy(offset, member).wait_send()
+
+
+def kernel_body(sizes, tokens, norm_gain, gate_weight, gate_scale, up_weight, up_scale, down_weight, down_scale):
+    n_rep, n_fs, n_tp = sizes
+    group = n_rep * n_tp
+    n_tok, width = tokens.shape
+    depth = gate_weight.shape[0]
+    units = gate_weight.shape[1] // n_rep
+    cols = down_weight.shape[1] // 2
+    first = lax.axis_index("rep") * units
+    own_gate = lax.dynamic_slice_in_dim(gate_weight, first, units, 1).astype(jnp.bfloat16)
+    own_up = lax.dynamic_slice_in_dim(up_weight, first, units, 1).astype(jnp.bfloat16)
+    own_down = lax.dynamic_slice_in_dim(down_weight, first, units, 0).astype(jnp.bfloat16)
+    own_gate_scale = lax.dynamic_slice_in_dim(gate_scale, first, units, 0)
+    own_up_scale = lax.dynamic_slice_in_dim(up_scale, first, units, 0)
+    vmem = pl.BlockSpec(memory_space=pltpu.VMEM)
+    anywhere = pl.BlockSpec(memory_space=pl.ANY)
+    steps = n_fs - 1
+    bf = jnp.bfloat16
+    dma = pltpu.SemaphoreType.DMA
+    return pl.pallas_call(
+        functools.partial(ffn_kernel, sizes),
+        out_shape=jax.ShapeDtypeStruct((n_tok, width), bf),
+        in_specs=[vmem, vmem, anywhere, vmem, anywhere, vmem, anywhere, vmem],
+        out_specs=vmem,
+        scratch_shapes=[
+            pltpu.VMEM((n_fs, depth, units), bf),
+            pltpu.VMEM((n_fs, depth, units), bf),
+            pltpu.VMEM((n_fs, 2, units, cols), bf),
+            pltpu.VMEM((group, n_tok, width), bf),
+            pltpu.VMEM((group, n_tok, units), jnp.float32),
+            pltpu.VMEM((group, n_tok, units), jnp.float32),
+            pltpu.VMEM((group, n_tok, units), bf),
+            pltpu.VMEM((2 * n_fs, group, n_tok, cols), bf),
+            pltpu.VMEM((2 * n_fs, group - 1, n_tok, cols), bf),
+            dma((4,)),
+            dma((2, 2, steps)), dma((2, 2, steps)),
+            dma((2, 2, steps)), dma((2, 2, steps)),
+            dma((group - 1,)), dma((group - 1,)),
+            dma((2 * n_fs, group - 1)), dma((2 * n_fs, group - 1)),
+        ],
+        compiler_params=pltpu.CompilerParams(
+            collective_id=0, has_side_effects=True, vmem_limit_bytes=62 * 1024 * 1024
+        ),
+    )(
+        tokens, norm_gain[None, :], own_gate, own_gate_scale[None, :], own_up, own_up_scale[None, :],
+        own_down, down_scale[None, :],
+    )
+
+
+def fits_kernel(mesh, tokens, gate_weight, down_weight):
+    n_rep, n_fs, n_tp = (mesh.shape[name] for name in ("rep", "fs", "tp"))
+    units = gate_weight.shape[1] // (n_tp * n_rep)
+    aligned = units % 128 == 0 and down_weight.shape[1] // n_fs % 256 == 0
+    return aligned and n_fs % 2 == 0 and n_fs >= 8 and n_rep * n_tp <= 4
+
+
 def solution(mesh):
-    return jax.shard_map(
-        body,
-        mesh=mesh,
-        in_specs=(
-            P(("rep", "fs", "tp"), None),
-            P(),
-            P("fs", "tp"),
-            P("tp"),
-            P("fs", "tp"),
-            P("tp"),
-            P("tp", "fs"),
-            P(),
-        ),
-        out_specs=P(("rep", "fs", "tp"), None),
-        check_vma=False,
-    )
+    sizes = tuple(mesh.shape[name] for name in ("rep", "fs", "tp"))
+
+    def run(tokens, norm_gain, gate_weight, gate_scale, up_weight, up_scale, down_weight, down_scale):
+        chosen = body
+        if fits_kernel(mesh, tokens, gate_weight, down_weight):
+            chosen = functools.partial(kernel_body, sizes)
+        return jax.shard_map(
+            chosen,
+            mesh=mesh,
+            in_specs=(
+                P(("rep", "fs", "tp"), None),
+                P(),
+                P("fs", "tp"),
+                P("tp"),
+                P("fs", "tp"),
+                P("tp"),
+                P("tp", "fs"),
+                P(),
+            ),
+            out_specs=P(("rep", "fs", "tp"), None),
+            check_vma=False,
+        )(tokens, norm_gain, gate_weight, gate_scale, up_weight, up_scale, down_weight, down_scale)
+
+    return run

time: 482 us -> 182 us (0.38)
  waiting for transfers between devices: 408 us -> 0 us
  Pallas kernels: 0 us -> 171 us
  matrix products: 43.9 us -> 0 us
  between operations: 14.6 us -> 0.01 us
    all_gather x4 -> x0, waiting for transfers between devices: 263 us -> none  [the longest x1 86.7 us: body(): lax.all_gather(own_down, 'fs', axis=1, tiled=True)]
    pallas_call x0 -> x1, Pallas kernels: none -> 171 us  [kernel_body(): pl.pallas_call(functools.partial(ffn_kernel, sizes), out_shape=jax.ShapeD...]
    ppermute x3 -> x0, waiting for transfers between devices: 133 us -> none  [from_partner(): lax.ppermute(shard, axis, [(i, i ^ 1 << distance) for i in range(lax.axis...]
    dot_general x2 -> x0, matrix products: 43.9 us -> none  [the longest x1 28.2 us: body(): jnp.dot(hidden, down_full, preferred_element_type=jnp.float32) * down_scale]
    reduce_scatter x1 -> x0, waiting for transfers between devices: 12.5 us -> none  [body(): lax.psum_scatter(partial_value.astype(jnp.float32).astype(jnp.bfloat16),...]
  transfers between devices with their start and end apart: 8 -> 0, of which waited for: 7 -> 0; matrix products, arithmetic and copies ran while one was open for 5% -> 0% of each run, Pallas kernels for 0% -> 0%
where the time goes in v1:
time: 182 us; the launch traced here: 181 us
  Pallas kernels  171 us (94%)
  local copies, waits for them, and re-layouts  10.2 us (6%)
    pallas_call x1, Pallas kernels, kernel_body(): pl.pallas_call(functools.partial(ffn_kernel, sizes), out_shape=jax.ShapeD...  171 us

profile of v1, /device:TPU:1, one launch (start us, length us, event | category | flops | bytes accessed | tf_op | source)
XLA Modules:
  0.0 181.2 jit_solution(2073629738333643644)
XLA Ops:
  0.0 0.8 dynamic_slice.16
  0.8 0.6 broadcast_in_dim.13.gscale_ref
  1.4 0.8 dynamic_slice.18
  2.2 0.6 broadcast_in_dim.14.uscale_ref
  2.8 2.2 %dynamic-slice_convert_fusion.down_ref = bf16[1280,256]{1,0:T(8,128)(2,1)} fusion(f32[2560,256]{1,0:T(8,128)} %param.14, s32[]{:T(128)S(6)} %select_n.2), kind=kLoop, calls=%fused_computation | loop fusion | bytes 1310724 | tf_op jit(solution)/shard_map/convert_element_type | solution.py:322
  5.0 2.9 %dynamic-slice_convert_fusion.1 = (bf16[256,1280]{1,0:T(8,128)(2,1)}, bf16[256,1280]{1,0:T(8,128)(2,1)}) fusion(f32[256,2560]{1,0:T(8,128)} %param.12, s32[]{:T(128)S(6)} %select_n.2, f32[256,2560]{1,0:T(8,128)} %param.10), kind=kLoop, calls=%fused_computation.1 | loop fusion | bytes 2621444 | tf_op jit(solution)/shard_map/convert_element_type | solution.py:321
  7.9 171.0 %shard_map.82 = bf16[256,2048]{1,0:T(8,128)(2,1)} custom-call(bf16[256,2048]{1,0:T(8,128)(2,1)} %tok_ref.1, f32[1,2048]{1,0:T(1,128)} %bitcast.2, bf16[256,1280]{1,0:T(8,128)(2,1)} %get-tuple-element.6.gate_ref, f32[1,1280]{1,0:T(1,128)} %broadcast_in_dim.13.gscale_ref, bf16[256,1280]{1,0:T(8,128)(2,1)} %get-tuple-element.5.up_ref, ...), custom_call_target="tpu_custom_call" | custom-call | tf_op jit(solution)/shard_map/pallas_call | solution.py:330
  178.9 2.3 %copy.10 = bf16[256,2048]{1,0:T(8,128)(2,1)} copy(bf16[256,2048]{1,0:T(8,128)(2,1)} %shard_map.82) | data formatting | bytes 2097152

commit v2 on v1

--- a/solution.py
+++ b/solution.py
@@ -70,7 +70,7 @@
 
 def ffn_kernel(
     sizes, tok_ref, gain_ref, gate_ref, gscale_ref, up_ref, uscale_ref, down_ref, dscale_ref, out_ref,
-    wg, wu, wd, rows_x, acc_g, acc_u, hid, staged, landed,
+    raw_g, raw_u, raw_d, wg, wu, wd, rows_x, acc_g, acc_u, hid, staged, landed,
     copy_sem, ring_send, ring_recv, down_send, down_recv, tok_send, tok_recv, part_send, part_recv,
 ):
     n_rep, n_fs, n_tp = sizes
@@ -147,29 +147,43 @@
             device_id=where, device_id_type=MESH,
         )
 
-    own = [
-        pltpu.make_async_copy(gate_ref, wg.at[fs], copy_sem.at[0]),
-        pltpu.make_async_copy(up_ref, wu.at[fs], copy_sem.at[1]),
-        pltpu.make_async_copy(down_ref.at[:, pl.ds(0, cols)], wd.at[fs, 0], copy_sem.at[2]),
-        pltpu.make_async_copy(down_ref.at[:, pl.ds(cols, cols)], wd.at[fs, 1], copy_sem.at[3]),
-    ]
-    for copy in own:
-        copy.start()
+    units = pl.ds(pl.multiple_of(rep * wg.shape[2], 128), wg.shape[2])
+    loads = []
+    for piece in range(2):
+        part = pl.ds(piece * half_depth, half_depth)
+        for direction, source, store in ((0, gate_ref, raw_g), (1, up_ref, raw_u)):
+            loads.append(
+                pltpu.make_async_copy(source.at[part, units], store.at[part], copy_sem.at[2 * piece + direction])
+            )
+    loads.append(pltpu.make_async_copy(down_ref.at[units], raw_d, copy_sem.at[4]))
+    for load in loads:
+        load.start()
     barrier = pltpu.get_barrier_semaphore()
     for device in [right, left] + [peer(offset)[1] for offset in range(1, group)]:
         pl.semaphore_signal(barrier, inc=1, device_id=device, device_id_type=MESH)
+
+    def round_piece(direction, piece):
+        loads[2 * piece + direction].wait()
+        part = slice(piece * half_depth, (piece + 1) * half_depth)
+        raw, store = (raw_g, wg) if direction == 0 else (raw_u, wu)
+        store[fs, part] = raw[part].astype(jnp.bfloat16)
+
+    round_piece(0, 0)
+    round_piece(1, 0)
     pl.semaphore_wait(barrier, group + 1)
-    own[0].wait()
-    own[1].wait()
-    for piece in range(2):
-        for direction in range(2):
-            ring_copy(direction, piece, 0).start()
+    ring_copy(0, 0, 0).start()
+    round_piece(0, 1)
+    ring_copy(1, 0, 0).start()
+    round_piece(1, 1)
+    ring_copy(0, 1, 0).start()
 
     values = tok_ref[...].astype(jnp.float32)
     inverse = lax.rsqrt(jnp.mean(values * values, axis=-1, keepdims=True) + EPS_VALUE)
     rows_x[member] = (values * inverse * gain_ref[...]).astype(jnp.bfloat16)
-    own[2].wait()
-    own[3].wait()
+    ring_copy(1, 1, 0).start()
+    loads[4].wait()
+    for direction in range(2):
+        wd[fs, direction] = raw_d[:, direction * cols:(direction + 1) * cols].astype(jnp.bfloat16)
     for offset in range(1, group):
         token_copy(offset, member).start()
 
@@ -197,49 +211,44 @@
         lax.fori_loop(0, group, tile, 0)
 
     def ring_step(step, carry):
-        for piece in range(2):
-            for direction in range(2):
-                ring_arrival(direction, piece, step).wait_recv()
-
-                @pl.when(step < steps - 1)
-                def _():
-                    ring_copy(direction, piece, step + 1).start()
-
         @pl.when(step == steps - 3)
         def _():
             for piece in range(2):
                 for direction in range(2):
                     down_copy(direction, piece, 0, 0).start()
 
-        @pl.when(step == half_ring - 1)
-        def _():
-            for offset in range(1, group):
-                token_copy(offset, (member + group - offset) % group).wait_recv()
-
-        @pl.when(step == steps - 1)
-        def _():
-            for piece in range(2):
+        def both(piece, inner):
+            for direction in range(2):
+                ring_arrival(direction, piece, step).wait_recv()
+
+                @pl.when(step < steps - 1)
+                def _():
+                    ring_copy(direction, piece, step + 1).start()
+
+            @pl.when(step == steps - 1)
+            def _():
                 for direction in range(2):
                     down_copy(direction, piece, 0, 1).wait_recv()
                     down_copy(direction, piece, 1, 1).start()
 
-        @pl.when(step >= half_ring - 1)
-        def _():
-            first = 2 * (step - (half_ring - 1))
-
-            def one(extra, inner):
-                add_slice(first + extra)
-                return inner
-
-            lax.fori_loop(0, 2, one, 0)
-
-        return carry
+            @pl.when((step == half_ring - 1) & (piece == 0))
+            def _():
+                for offset in range(1, group):
+                    token_copy(offset, (member + group - offset) % group).wait_recv()
+
+            @pl.when(step >= half_ring - 1)
+            def _():
+                add_slice(2 * (step - (half_ring - 1)) + piece)
+
+            return inner
+
+        return lax.fori_loop(0, 2, both, carry)
 
     lax.fori_loop(0, steps, ring_step, 0)
 
     def activate(block, carry):
-        gate_pre = acc_g[block] * gscale_ref[...]
-        up_pre = acc_u[block] * uscale_ref[...]
+        gate_pre = acc_g[block] * gscale_ref[:, units]
+        up_pre = acc_u[block] * uscale_ref[:, units]
         hid[block] = (jax.nn.silu(gate_pre) * up_pre).astype(jnp.bfloat16)
         return carry
 
@@ -252,7 +261,8 @@
             scale = dscale_ref[:, pl.ds(start, cols)]
             index = 2 * hops + direction
 
-            def tile(block, carry):
+            def tile(turn, carry):
+                block = (member + 1 + turn) % group
                 product = jnp.dot(hid[block], wd[source, direction], preferred_element_type=jnp.float32)
                 staged[index, block] = (product * scale).astype(jnp.bfloat16)
                 return carry
@@ -262,20 +272,25 @@
                 part_copy(offset, index).start()
 
     def down_step(step, carry):
-        @pl.when((step >= 2) & (step <= steps))
-        def _():
-            for piece in range(2):
-                for direction in range(2):
-                    down_copy(direction, piece, step - 1, step).wait_recv()
-
-                    @pl.when(step < steps)
-                    def _():
-                        down_copy(direction, piece, step, step).start()
-
-        produce(step)
-        return carry
-
-    lax.fori_loop(0, n_fs, down_step, 0)
+        hops = step + 2
+        for piece in range(2):
+            for direction in range(2):
+                down_copy(direction, piece, hops - 1, hops).wait_recv()
+
+                @pl.when(hops < steps)
+                def _():
+                    down_copy(direction, piece, hops, hops).start()
+
+        low = step + 2 * ((step // 2 + n_fs - 1) // n_fs)
+        high = step + 1 + 2 * ((step + n_fs - 1) // n_fs)
+
+        def one(done_hops, inner):
+            produce(done_hops)
+            return inner
+
+        return lax.fori_loop(low, high, one, carry)
+
+    lax.fori_loop(0, n_fs - 2, down_step, 0)
 
     def finish(hops, carry):
         for direction in range(2):
@@ -316,12 +331,6 @@
     depth = gate_weight.shape[0]
     units = gate_weight.shape[1] // n_rep
     cols = down_weight.shape[1] // 2
-    first = lax.axis_index("rep") * units
-    own_gate = lax.dynamic_slice_in_dim(gate_weight, first, units, 1).astype(jnp.bfloat16)
-    own_up = lax.dynamic_slice_in_dim(up_weight, first, units, 1).astype(jnp.bfloat16)
-    own_down = lax.dynamic_slice_in_dim(down_weight, first, units, 0).astype(jnp.bfloat16)
-    own_gate_scale = lax.dynamic_slice_in_dim(gate_scale, first, units, 0)
-    own_up_scale = lax.dynamic_slice_in_dim(up_scale, first, units, 0)
     vmem = pl.BlockSpec(memory_space=pltpu.VMEM)
     anywhere = pl.BlockSpec(memory_space=pl.ANY)
     steps = n_fs - 1
@@ -333,6 +342,9 @@
         in_specs=[vmem, vmem, anywhere, vmem, anywhere, vmem, anywhere, vmem],
         out_specs=vmem,
         scratch_shapes=[
+            pltpu.VMEM((depth, units), jnp.float32),
+            pltpu.VMEM((depth, units), jnp.float32),
+            pltpu.VMEM((units, 2 * cols), jnp.float32),
             pltpu.VMEM((n_fs, depth, units), bf),
             pltpu.VMEM((n_fs, depth, units), bf),
             pltpu.VMEM((n_fs, 2, units, cols), bf),
@@ -342,7 +354,7 @@
             pltpu.VMEM((group, n_tok, units), bf),
             pltpu.VMEM((2 * n_fs, group, n_tok, cols), bf),
             pltpu.VMEM((2 * n_fs, group - 1, n_tok, cols), bf),
-            dma((4,)),
+            dma((5,)),
             dma((2, 2, steps)), dma((2, 2, steps)),
             dma((2, 2, steps)), dma((2, 2, steps)),
             dma((group - 1,)), dma((group - 1,)),
@@ -352,8 +364,8 @@
             collective_id=0, has_side_effects=True, vmem_limit_bytes=62 * 1024 * 1024
         ),
     )(
-        tokens, norm_gain[None, :], own_gate, own_gate_scale[None, :], own_up, own_up_scale[None, :],
-        own_down, down_scale[None, :],
+        tokens, norm_gain[None, :], gate_weight, gate_scale[None, :], up_weight, up_scale[None, :],
+        down_weight, down_scale[None, :],
     )
 
 

time: 182 us -> 175 us (0.962)
  local copies, waits for them, and re-layouts: 10.2 us -> 4.92 us
    convert_element_type x2 -> x0, local copies, waits for them, and re-layouts: 5.15 us -> none  [the longest x1 2.91 us: kernel_body(): lax.dynamic_slice_in_dim(up_weight, first, units, 1).astype(jnp.bfloat16)]
where the time goes in v2:
time: 175 us
  Pallas kernels  170 us (97%)
  local copies, waits for them, and re-layouts  4.92 us (3%)
    pallas_call x1, Pallas kernels, kernel_body(): pl.pallas_call(functools.partial(ffn_kernel, sizes), out_shape=jax.ShapeD...  170 us

profile of v2, /device:TPU:1, one launch (start us, length us, event | category | flops | bytes accessed | tf_op | source)
XLA Modules:
  0.0 175.1 jit_solution(4668416480211982253)
XLA Ops:
  0.0 1.3 broadcast_in_dim.13.gscale_ref
  1.3 1.3 broadcast_in_dim.14.uscale_ref
  2.6 170.2 %shard_map.82 = bf16[256,2048]{1,0:T(8,128)(2,1)} custom-call(bf16[256,2048]{1,0:T(8,128)(2,1)} %tok_ref.1, f32[1,2048]{1,0:T(1,128)} %bitcast.2, f32[256,2560]{1,0:T(8,128)} %gate_ref.1, f32[1,2560]{1,0:T(1,128)} %broadcast_in_dim.13.gscale_ref, f32[256,2560]{1,0:T(8,128)} %up_ref.1, f32[1,2560]{1,0:T(1,128)} %broadcast_in_dim.14.uscale_ref, ...), custom_call_target="tpu_custom_call" | custom-call | tf_op jit(solution)/shard_map/pallas_call | solution.py:339
  172.8 2.3 %copy.10 = bf16[256,2048]{1,0:T(8,128)(2,1)} copy(bf16[256,2048]{1,0:T(8,128)(2,1)} %shard_map.82) | data formatting | bytes 2097152
